TPU v7x, 32 devices: a whole 2x2x4 slice. The times are simulated.
32 devices in a mesh: grp: 2 (over y), sp: 4 (over z), tp: 4 (over x, core).
Axes of the slice: x: 2, y: 2, z: 4, core: 2. Of those that a mesh axis runs over, the one named last changes fastest.
Arguments:
- latent: bfloat16 [1024, 2048], P(('grp', 'sp', 'tp')), parts along dimension 0, may hold values from -6 to 6
- context: bfloat16 [512, 2048], P(('grp', 'sp')), parts along dimension 0, may hold values from -6 to 6
- condition: float32 [4096], P('grp'), parts along dimension 0, may hold values from -6 to 6
- ctx_condition: float32 [2048], replicated, may hold values from -6 to 6
- w_mod: bfloat16 [2048, 6144], P('sp', 'tp'), may hold values from -0.125 to 0.125
- w_recept: bfloat16 [2048, 1024], P('sp', 'tp'), may hold values from -0.125 to 0.125
- w_key: bfloat16 [2048, 1024], P('sp', 'tp'), may hold values from -0.125 to 0.125
- w_value: bfloat16 [2048, 1024], P('sp', 'tp'), may hold values from -0.125 to 0.125
- w_decay_down: bfloat16 [2048, 64], replicated, may hold values from -0.125 to 0.125
- w_decay_up: bfloat16 [64, 1024], P(None, 'tp'), may hold values from -0.75 to 0.75
- decay_base: float32 [1024], P('tp'), may hold values from -12 to -3.5
- decay_shift: float32 [1024, 16], P(('grp', 'sp'), 'tp'), parts along dimension 0, may hold values from -1 to 26
- w_rate_down: bfloat16 [2048, 64], replicated, may hold values from -0.125 to 0.125
- w_rate_up: bfloat16 [64, 1024], P(None, 'tp'), may hold values from -0.75 to 0.75
- rate_bias: float32 [1024], P('tp'), may hold values from -8 to -1
- w_out: bfloat16 [1024, 2048], P('tp'), may hold values from -0.1875 to 0.1875
Outputs:
- mixed: bfloat16 [1024, 2048], P(('grp', 'sp', 'tp')), parts along dimension 0
There are 2 independent parts, one for each index of `grp`. A program takes and returns all parts, laid end to end along the dimension named above; an argument that names none is the same for every part. Nothing has to cross between parts.
All inputs are finite; a program needn't handle non-finite values.
Results may differ from a plain program's by a relative error of at most 0.011.
Values may be sent and summed in bfloat16 or wider, within the bound.
A program may use at most 64 MiB of HBM per device.

v0:
```python
import jax
import jax.numpy as jnp
from jax import lax
from jax.sharding import PartitionSpec as P

HEAD = 64
BLOCK = 64


NORM_EPS = 1e-06
HEAD_EPS = 0.00064
DECAY_SCALE = 0.6065306597126334
EXACT_MODE = lax.Precision.HIGHEST


def carried_in(x, axis, combine, identity, reverse):
    length, position = (lax.axis_size(axis), lax.axis_index(axis))
    everything = jax.tree.map(
        lambda part, kind: lax.all_gather(part.astype(kind), axis), x, (jnp.bfloat16, jnp.bfloat16)
    )
    start = jax.tree.map(
        lambda part, zero: jnp.broadcast_to(jnp.asarray(zero, part.dtype), part.shape), x, identity
    )

    def hop(k, before):
        at = length - 1 - k if reverse else k
        reached = at > position if reverse else at < position
        new = combine(
            before, jax.tree.map(lambda part, own: part[at].astype(own.dtype), everything, x)
        )
        return jax.tree.map(lambda a, b: jnp.where(reached, a, b), new, before)

    return lax.fori_loop(0, length, hop, start)


def matmul(lhs_matrix, rhs_matrix):
    return jnp.dot(lhs_matrix, rhs_matrix, preferred_element_type=jnp.float32)


def stored(matrix):
    return lax.optimization_barrier(matrix.astype(jnp.bfloat16))


def modulate(row_block, shift_row, scale_row):
    values = row_block.astype(jnp.float32)
    normed = values * lax.rsqrt(jnp.mean(values * values, axis=-1, keepdims=True) + NORM_EPS)
    return (normed * (1.0 + scale_row) + shift_row).astype(jnp.bfloat16)


def to_heads(matrix):
    tokens = matrix.shape[0]
    return jnp.transpose(matrix.astype(jnp.float32).reshape(tokens, -1, HEAD), (1, 0, 2))


def gate_terms(decay_low, rate_low, w_decay_up, decay_base, w_rate_up, rate_bias):
    squashed = jnp.tanh(decay_low.astype(jnp.float32)).astype(jnp.bfloat16)
    pre_decay = decay_base + matmul(squashed, w_decay_up)
    rate_gate = jax.nn.sigmoid(rate_bias + matmul(rate_low, w_rate_up))
    return (pre_decay, rate_gate)


def unit_lower_inverse(strict):
    block_len = strict.shape[-1]
    identity = jnp.eye(block_len, dtype=jnp.float32)
    inverse = identity - strict
    squared = strict
    for doubling in range((block_len - 1).bit_length() - 1):
        squared = jnp.einsum("hij,hjk->hik", squared, squared, precision=EXACT_MODE)
        inverse = jnp.einsum("hij,hjk->hik", inverse, identity + squared, precision=EXACT_MODE)
    return inverse


def block_pass(memory, pieces, with_output):
    key_rows, value_rows, log_decay, rate_rows, receive = pieces
    block_len = key_rows.shape[1]
    padding = memory.shape[1] - value_rows.shape[2]
    kappa_rows = key_rows * lax.rsqrt(
        jnp.sum(key_rows * key_rows, axis=-1, keepdims=True) + NORM_EPS
    )
    beta_rows = kappa_rows * rate_rows
    cumulative = jnp.cumsum(log_decay, axis=1)
    previous = cumulative - log_decay
    centre = cumulative[:, block_len // 2 - 1 : block_len // 2, :]
    inward = jnp.exp(centre - cumulative)
    key_in = key_rows * inward
    beta_in = beta_rows * inward
    kappa_out = kappa_rows * jnp.exp(previous - centre)
    strict = jnp.tril(jnp.ones((block_len, block_len), jnp.float32), -1)
    beta_mix = jnp.einsum("hlc,hmc->hlm", kappa_out, beta_in, precision=EXACT_MODE) * strict
    key_mix = jnp.einsum("hlc,hmc->hlm", kappa_out, key_in, precision=EXACT_MODE) * strict
    pushed = jnp.einsum("hlm,hmv->hlv", key_mix, value_rows, precision=EXACT_MODE)
    target = jnp.einsum(
        "hvc,hlc->hlv", memory, kappa_rows * jnp.exp(previous), precision=EXACT_MODE
    )
    target = target + jnp.pad(pushed, ((0, 0), (0, 0), (padding, 0)))
    removed = jnp.einsum("hlm,hmv->hlv", unit_lower_inverse(beta_mix), target, precision=EXACT_MODE)
    closing = cumulative[:, block_len - 1 :, :]
    remain = jnp.exp(closing - cumulative)
    written = jnp.einsum("hlv,hlc->hvc", value_rows, key_rows * remain, precision=EXACT_MODE)
    new_state = memory * jnp.exp(closing) + jnp.pad(written, ((0, 0), (padding, 0), (0, 0)))
    new_state = new_state - jnp.einsum(
        "hlv,hlc->hvc", removed, beta_rows * remain, precision=EXACT_MODE
    )
    if not with_output:
        return (new_state, None)
    inclusive = jnp.tril(jnp.ones((block_len, block_len), jnp.float32))
    read_rows = receive * jnp.exp(cumulative - centre)
    read_key = jnp.einsum("hlc,hmc->hlm", read_rows, key_in, precision=EXACT_MODE) * inclusive
    read_beta = jnp.einsum("hlc,hmc->hlm", read_rows, beta_in, precision=EXACT_MODE) * inclusive
    carried = jnp.einsum(
        "hvc,hlc->hlv", memory, receive * jnp.exp(cumulative), precision=EXACT_MODE
    )
    local_part = jnp.einsum("hlm,hmv->hlv", read_key, value_rows, precision=EXACT_MODE)
    output = carried + jnp.pad(local_part, ((0, 0), (0, 0), (padding, 0)))
    output = output - jnp.einsum("hlm,hmv->hlv", read_beta, removed, precision=EXACT_MODE)
    return (new_state, output)


def run_blocks(memory, pieces, with_output):

    def split_blocks(tensor):
        head_count, tokens, channels = tensor.shape
        return jnp.moveaxis(tensor.reshape(head_count, tokens // BLOCK, BLOCK, channels), 1, 0)

    stacked = jax.tree.map(split_blocks, pieces)

    def advance(running, block_pieces):
        return block_pass(running, block_pieces, with_output)

    last_state, outputs = lax.scan(advance, memory, stacked)
    if with_output:
        block_count, head_count, block_len, state_rows = outputs.shape
        outputs = jnp.moveaxis(outputs, 0, 1).reshape(
            head_count, block_count * block_len, state_rows
        )
    return (last_state, outputs)


def flip_tokens(pieces):
    return jax.tree.map(lambda tensor: jnp.flip(tensor, axis=1), pieces)


def compose(earlier_map, later_map):
    joined_decay = jnp.einsum("hij,hjk->hik", earlier_map[0], later_map[0], precision=EXACT_MODE)
    joined_write = (
        jnp.einsum("hij,hjk->hik", earlier_map[1], later_map[0], precision=EXACT_MODE)
        + later_map[1]
    )
    return (joined_decay, joined_write)


def resolve(entering, augmented):
    return (
        jnp.einsum("hvc,htc->htv", entering, augmented[:, :, :HEAD], precision=EXACT_MODE)
        + augmented[:, :, HEAD:]
    )


def shards(
    latent,
    context,
    condition,
    ctx_condition,
    w_mod,
    w_recept,
    w_key,
    w_value,
    w_decay_down,
    w_decay_up,
    decay_base,
    decay_shift,
    w_rate_down,
    w_rate_up,
    rate_bias,
    w_out,
):
    model_width = latent.shape[1]
    row_slab = w_mod.shape[0]
    conditions = jax.nn.silu(jnp.stack([condition, ctx_condition])).astype(jnp.bfloat16)
    activated = lax.dynamic_slice_in_dim(conditions, lax.axis_index("sp") * row_slab, row_slab, 1)
    partial_mod = matmul(activated, w_mod)
    summed = lax.psum(partial_mod, "sp")
    modulation = lax.all_gather(summed, "tp", axis=1, tiled=True)
    shift_rows = modulation[:, :model_width]
    scale_rows = modulation[:, model_width : 2 * model_width]
    gate_row = modulation[0, 2 * model_width :]
    hidden_lat = modulate(latent, shift_rows[0], scale_rows[0])
    hidden_ctx = modulate(context, shift_rows[1], scale_rows[1])
    lat_rows = lax.all_gather(hidden_lat, "tp", axis=0, tiled=True)
    tok_count = lat_rows.shape[0]
    columns = w_recept.shape[1]
    recept_piece = lax.all_gather(w_recept, "sp", axis=0, tiled=True)
    key_piece = lax.all_gather(w_key, "sp", axis=0, tiled=True)
    value_piece = lax.all_gather(w_value, "sp", axis=0, tiled=True)
    recept_lat = matmul(lat_rows, recept_piece)
    key_lat = matmul(lat_rows, key_piece)
    value_lat = matmul(lat_rows, value_piece)
    key_ctx = matmul(hidden_ctx, key_piece)
    value_ctx = matmul(hidden_ctx, value_piece)
    decay_lat = stored(matmul(lat_rows, w_decay_down))
    rate_lat = stored(matmul(lat_rows, w_rate_down))
    key_ctx = stored(key_ctx)
    value_ctx = stored(value_ctx)
    decay_ctx = stored(matmul(hidden_ctx, w_decay_down))
    rate_ctx = stored(matmul(hidden_ctx, w_rate_down))
    key_ctx, value_ctx, decay_ctx, rate_ctx = (
        lax.all_gather(key_ctx, "sp", axis=0, tiled=True),
        lax.all_gather(value_ctx, "sp", axis=0, tiled=True),
        lax.all_gather(decay_ctx, "sp", axis=0, tiled=True),
        lax.all_gather(rate_ctx, "sp", axis=0, tiled=True),
    )
    pre_lat, gate_lat = gate_terms(
        decay_lat, rate_lat, w_decay_up, decay_base, w_rate_up, rate_bias
    )
    pre_ctx, gate_ctx = gate_terms(
        decay_ctx, rate_ctx, w_decay_up, decay_base, w_rate_up, rate_bias
    )
    log_lat = -DECAY_SCALE * jax.nn.sigmoid(
        to_heads(pre_lat) + jnp.transpose(decay_shift)[:, :, None]
    )
    log_ctx = -DECAY_SCALE * jax.nn.sigmoid(to_heads(pre_ctx))
    lat_pieces = (
        to_heads(stored(key_lat)),
        to_heads(stored(value_lat)),
        log_lat,
        to_heads(gate_lat),
        to_heads(stored(recept_lat)),
    )
    ctx_pieces = (to_heads(key_ctx), to_heads(value_ctx), log_ctx, to_heads(gate_ctx), None)
    heads_dev = columns // HEAD
    zero_state = jnp.zeros((heads_dev, HEAD, HEAD), jnp.float32)
    ctx_forward, _ = run_blocks(zero_state, ctx_pieces, False)
    ctx_backward, _ = run_blocks(zero_state, flip_tokens(ctx_pieces), False)
    eye_block = jnp.broadcast_to(jnp.eye(HEAD, dtype=jnp.float32), (heads_dev, HEAD, HEAD))
    start_state = jnp.concatenate([eye_block, zero_state], axis=1)
    fwd_map, fwd_out = run_blocks(start_state, lat_pieces, True)
    bwd_map, bwd_flipped = run_blocks(start_state, flip_tokens(lat_pieces), True)
    bwd_out = jnp.flip(bwd_flipped, axis=1)
    neutral = (eye_block, zero_state)
    before_map = carried_in((fwd_map[:, :HEAD], fwd_map[:, HEAD:]), "sp", compose, neutral, False)
    after_map = carried_in((bwd_map[:, :HEAD], bwd_map[:, HEAD:]), "sp", compose, neutral, True)
    enter_fwd = (
        jnp.einsum("hij,hjk->hik", ctx_forward, before_map[0], precision=EXACT_MODE) + before_map[1]
    )
    enter_bwd = (
        jnp.einsum("hij,hjk->hik", ctx_backward, after_map[0], precision=EXACT_MODE) + after_map[1]
    )
    mixed_heads = resolve(enter_fwd, fwd_out) + resolve(enter_bwd, bwd_out)
    centred = mixed_heads - jnp.mean(mixed_heads, axis=-1, keepdims=True)
    normed = centred * lax.rsqrt(jnp.mean(centred * centred, axis=-1, keepdims=True) + HEAD_EPS)
    normed_rows = jnp.transpose(normed, (1, 0, 2)).reshape(tok_count, columns).astype(jnp.bfloat16)
    branch = lax.psum_scatter(
        matmul(normed_rows, w_out).astype(jnp.bfloat16), "tp", scatter_dimension=0, tiled=True
    )
    rounded = lax.optimization_barrier(branch).astype(jnp.float32)
    return (latent.astype(jnp.float32) + gate_row * rounded).astype(jnp.bfloat16)


def solution(mesh):
    return jax.shard_map(
        shards,
        mesh=mesh,
        in_specs=(
            P(("grp", "sp", "tp"), None),
            P(("grp", "sp"), None),
            P("grp"),
            P(),
            P("sp", "tp"),
            P("sp", "tp"),
            P("sp", "tp"),
            P("sp", "tp"),
            P(),
            P(None, "tp"),
            P("tp"),
            P(("grp", "sp"), "tp"),
            P(),
            P(None, "tp"),
            P("tp"),
            P("tp", None),
        ),
        out_specs=P(("grp", "sp", "tp"), None),
        check_vma=False,
    )
```

profile of v0, /device:TPU:1, one launch (start us, length us, event | category | flops | bytes accessed | tf_op | source)
XLA Modules:
  0.0 363.4 jit_solution(3352462058849512410)
XLA Ops:
  9.9 16.6 %psum.7 = f32[2,1536]{1,0:T(2,128)S(1)} all-reduce(f32[2,1536]{1,0:T(2,128)S(1)} %fusion.186), channel_id=1, replica_groups=mesh['grp'=2,'sp'=4,'tp'=4] {'sp'}, use_global_device_ids=true, to_apply=%region_0.1 | all-reduce | flops 3072 | bytes 24576 | tf_op jit(solution)/shard_map/psum | solution.py:182
  26.6 9.6 %all_gather.51 = f32[2,6144]{1,0:T(2,128)S(1)} all-gather(f32[2,1536]{1,0:T(2,128)S(1)} %psum.7), channel_id=1, replica_groups=mesh['grp'=2,'sp'=4,'tp'=4] {'tp'}, dimensions={1}, use_global_device_ids=true | all-gather | bytes 61440 | tf_op jit(solution)/shard_map/all_gather | solution.py:183
  36.5 7.3 %all_gather.52 = bf16[128,2048]{1,0:T(8,128)(2,1)S(1)} all-gather(bf16[32,2048]{1,0:T(8,128)(2,1)S(1)} %fusion.180), channel_id=1, replica_groups=mesh['grp'=2,'sp'=4,'tp'=4] {'tp'}, dimensions={0}, use_global_device_ids=true | all-gather | bytes 655360 | tf_op jit(solution)/shard_map/all_gather | solution.py:189
  48.4 11.1 %all_gather.59 = bf16[256,64]{1,0:T(8,128)(2,1)S(1)} all-gather(bf16[64,64]{1,0:T(8,128)(2,1)S(1)} %convolution_convert_fusion.8), channel_id=1, replica_groups=mesh['grp'=2,'sp'=4,'tp'=4] {'sp'}, dimensions={0}, use_global_device_ids=true | all-gather | bytes 40960 | tf_op jit(solution)/shard_map/all_gather | solution.py:210
  62.6 1.8 reshape.289
  66.5 10.4 %all_gather.56 = bf16[256,64]{1,0:T(8,128)(2,1)S(1)} all-gather(bf16[64,64]{1,0:T(8,128)(2,1)S(1)} %convolution_convert_fusion.9), channel_id=1, replica_groups=mesh['grp'=2,'sp'=4,'tp'=4] {'sp'}, dimensions={0}, use_global_device_ids=true | all-gather | bytes 40960 | tf_op jit(solution)/shard_map/all_gather | solution.py:209
  78.1 1.7 divide_multiply_fusion
  79.8 2.0 reshape.295
  81.8 2.0 reshape.298
  85.4 2.0 reshape.282
  87.4 1.5 convolution_convert_fusion.3
  90.0 1.5 convolution_convert_fusion.2
  93.3 4.6 %all-gather.12.cloned.1.call-done = bf16[2048,256]{1,0:T(8,128)(2,1)} async-done(((bf16[512,256]{1,0:T(8,128)(2,1)}), bf16[2048,256]{1,0:T(8,128)(2,1)}) %all-gather.12.cloned.1.call-update) | async-done | bytes 1048592 | tf_op jit(solution)/shard_map/all_gather | solution.py:192
  97.9 1.5 convolution_convert_fusion.1
  100.6 1.6 convolution_convert_fusion.5
  102.1 10.6 %all_gather.57 = bf16[256,256]{1,0:T(8,128)(2,1)S(1)} all-gather(bf16[64,256]{1,0:T(8,128)(2,1)S(1)} %convolution_convert_fusion.5), channel_id=1, replica_groups=mesh['grp'=2,'sp'=4,'tp'=4] {'sp'}, dimensions={0}, use_global_device_ids=true | all-gather | bytes 163840 | tf_op jit(solution)/shard_map/all_gather | solution.py:208
  114.8 1.6 convolution_convert_fusion.4
  116.4 10.6 %all_gather.58 = bf16[256,256]{1,0:T(8,128)(2,1)S(1)} all-gather(bf16[64,256]{1,0:T(8,128)(2,1)S(1)} %convolution_convert_fusion.4), channel_id=1, replica_groups=mesh['grp'=2,'sp'=4,'tp'=4] {'sp'}, dimensions={0}, use_global_device_ids=true | all-gather | bytes 163840 | tf_op jit(solution)/shard_map/all_gather | solution.py:207
  131.8 24.5 %while.85 = (s32[]{:T(128)}, f32[4,128,64]{1,2,0:T(8,128)S(1)}, f32[2,4,64,128]{3,2,0,1:T(8,128)}, f32[2,4,64,64]{2,0,3,1:T(2,128)}, f32[2,4,64,64]{2,0,3,1:T(2,...) while((s32[]{:T(128)}, f32[4,128,64]{1,2,0:T(8,128)S(1)}, ...), condition=%wide.region_16.17_spmd, body=%wide.region_13.16_spmd.sunk | while | flops 341745728 | bytes 8541357 | solution.py:130
  156.5 10.9 %all-gather.2 = bf16[16,64,64]{2,1,0:T(8,128)(2,1)S(1)} all-gather(bf16[4,64,64]{2,1,0:T(8,128)(2,1)S(1)} %get-tuple-element.813), channel_id=4, replica_groups=mesh['grp'=2,'sp'=4,'tp'=4] {'sp'}, dimensions={0}, use_global_device_ids=true | all-gather | bytes 163840 | tf_op jit(solution)/shard_map/all_gather | solution.py:19
  167.4 12.4 %all-gather.3 = bf16[16,64,64]{2,1,0:T(8,128)(2,1)S(1)} all-gather(bf16[4,64,64]{2,1,0:T(8,128)(2,1)S(1)} %get-tuple-element.812), channel_id=5, replica_groups=mesh['grp'=2,'sp'=4,'tp'=4] {'sp'}, dimensions={0}, use_global_device_ids=true | all-gather | bytes 163840 | tf_op jit(solution)/shard_map/all_gather | solution.py:19
  179.8 3.0 while.89
  184.6 2.0 reshape.297
  186.6 35.7 %while.88 = (s32[]{:T(128)}, f32[4,64,64]{2,1,0:T(8,128)S(1)}, f32[4,4,64,64]{2,0,3,1:T(4,128)}, f32[4,4,64,64]{2,0,3,1:T(4,128)}, f32[4,4,64,64]{2,0,3,1:T(4,12...) while((s32[]{:T(128)}, f32[4,64,64]{2,1,0:T(8,128)S(1)}, ...), condition=%wide.region_20.21_spmd.clone, body=%wide.region_17.20_spmd.clone.sunk | while | flops 215597120 | bytes 5015156 | solution.py:130
  223.0 24.3 %while.84 = (s32[]{:T(128)}, f32[4,128,64]{1,2,0:T(8,128)S(1)}, f32[2,4,64,128]{3,2,0,1:T(8,128)}, f32[2,4,64,64]{2,0,3,1:T(2,128)}, f32[2,4,64,64]{2,0,3,1:T(2,...) while((s32[]{:T(128)}, f32[4,128,64]{1,2,0:T(8,128)S(1)}, ...), condition=%wide.region_5.6_spmd, body=%wide.region_2.5_spmd.sunk | while | flops 341745728 | bytes 7492725 | solution.py:130
  247.5 11.2 %all-gather = bf16[16,64,64]{2,1,0:T(8,128)(2,1)S(1)} all-gather(bf16[4,64,64]{2,1,0:T(8,128)(2,1)S(1)} %get-tuple-element.815), channel_id=2, replica_groups=mesh['grp'=2,'sp'=4,'tp'=4] {'sp'}, dimensions={0}, use_global_device_ids=true | all-gather | bytes 163840 | tf_op jit(solution)/shard_map/all_gather | solution.py:19
  258.7 11.2 %all-gather.1 = bf16[16,64,64]{2,1,0:T(8,128)(2,1)S(1)} all-gather(bf16[4,64,64]{2,1,0:T(8,128)(2,1)S(1)} %get-tuple-element.814), channel_id=3, replica_groups=mesh['grp'=2,'sp'=4,'tp'=4] {'sp'}, dimensions={0}, use_global_device_ids=true | all-gather | bytes 163840 | tf_op jit(solution)/shard_map/all_gather | solution.py:19
  269.9 2.9 while.87
  273.6 35.6 %while.86 = (s32[]{:T(128)}, f32[4,64,64]{2,1,0:T(8,128)S(1)}, f32[4,4,64,64]{2,0,3,1:T(4,128)}, f32[4,4,64,64]{2,0,3,1:T(4,128)}, f32[4,4,64,64]{2,0,3,1:T(4,12...) while((s32[]{:T(128)}, f32[4,64,64]{2,1,0:T(8,128)S(1)}, ...), condition=%wide.region_10.11_spmd.clone, body=%wide.region_7.10_spmd.clone.sunk | while | flops 215597120 | bytes 5015156 | solution.py:130
  311.2 1.8 slice.101
  317.4 37.9 %reduce-scatter.2.cloned.1.call-done = bf16[32,2048]{1,0:T(8,128)(2,1)} async-done(((bf16[128,2048]{1,0:T(8,128)(2,1)}), bf16[32,2048]{1,0:T(8,128)(2,1)}) %reduce-scatter.2.cloned.1.call-update) | async-done | bytes 131088 | tf_op jit(solution)/shard_map/reduce_scatter | solution.py:252
  355.3 1.6 fusion.181
  (562 shorter events, 159.5 us)
Async XLA Ops:
  6.5 2.3 copy-start
  6.5 29.7 %copy-start.9 = (bf16[32,2048]{1,0:T(8,128)(2,1)S(1)}, bf16[32,2048]{1,0:T(8,128)(2,1)}, u32[]{:S(2)}) copy-start(bf16[32,2048]{1,0:T(8,128)(2,1)} %param.28) | copy-start | bytes 393220
  6.5 80.9 %all-gather.8.cloned.1.call-start = ((), (), s32[]{:S(2)}) async-start(), calls=%async_computation.1 | async-start | bytes 1310720 | tf_op jit(solution)/shard_map/all_gather | solution.py:194
  7.3 82.8 %all-gather.10.cloned.1.call-start = ((), (), s32[]{:S(2)}) async-start(), calls=%async_computation.2 | async-start | bytes 1310720 | tf_op jit(solution)/shard_map/all_gather | solution.py:193
  8.0 35.8 %copy-start.15 = (bf16[2048,64]{0,1:T(8,128)(2,1)S(1)}, bf16[2048,64]{0,1:T(8,128)(2,1)}, u32[]{:S(2)}) copy-start(bf16[2048,64]{0,1:T(8,128)(2,1)} %param.40) | copy-start | bytes 786436
  8.0 89.9 %all-gather.12.cloned.1.call-start = ((), (), s32[]{:S(2)}) async-start(), calls=%async_computation.3 | async-start | bytes 1310720 | tf_op jit(solution)/shard_map/all_gather | solution.py:192
  8.8 346.6 %reduce-scatter.2.cloned.1.call-start = ((), (), s32[]{:S(2)}) async-start(), calls=%async_computation.4 | async-start | bytes 655360 | tf_op jit(solution)/shard_map/reduce_scatter | solution.py:252
  8.8 35.2 %copy-start.19 = (bf16[64,256]{1,0:T(8,128)(2,1)S(1)}, bf16[64,256]{1,0:T(8,128)(2,1)}, u32[]{:S(2)}) copy-start(bf16[64,256]{1,0:T(8,128)(2,1)} %param.41) | copy-start | bytes 98308
  8.9 35.2 %copy-start.20 = (f32[256]{0:T(256)S(1)}, f32[256]{0:T(256)}, u32[]{:S(2)}) copy-start(f32[256]{0:T(256)} %param.42) | copy-start | bytes 3076
  43.8 2.9 copy-start.16
  43.8 3.0 copy-start.17
  43.8 3.3 copy-start.18
  44.3 3.6 copy-start.6
  60.6 6.0 %copy-start.1 = (f32[4,128,64]{1,2,0:T(8,128)}, f32[4,128,64]{1,2,0:T(8,128)S(1)}, u32[]{:S(2)}) copy-start(f32[4,128,64]{1,2,0:T(8,128)S(1)} %concatenate.3) | copy-start | bytes 393220
  114.8 14.5 %copy-start.13 = (f32[4,128,64]{1,2,0:T(8,128)S(1)}, f32[4,128,64]{1,2,0:T(8,128)}, u32[]{:S(2)}) copy-start(f32[4,128,64]{1,2,0:T(8,128)} %rev.33) | copy-start | bytes 393220
  127.0 4.8 %copy-start.3 = (f32[4,128,64]{1,2,0:T(8,128)S(1)}, f32[4,128,64]{1,2,0:T(8,128)}, u32[]{:S(2)}) copy-start(f32[4,128,64]{1,2,0:T(8,128)} %copy-done.1) | copy-start | bytes 393220
  131.8 3.7 %copy-start.4 = (f32[2,4,64,64]{2,0,3,1:T(2,128)}, f32[2,4,64,64]{2,0,3,1:T(2,128)S(1)}, u32[]{:S(2)}) copy-start(f32[2,4,64,64]{2,0,3,1:T(2,128)S(1)} %get-tuple-element.1230) | copy-start | bytes 393220 | tf_op jit(solution)/shard_map/while
  141.6 2.5 copy-start.5
  144.1 3.7 %copy-start.4 = (f32[2,4,64,64]{2,0,3,1:T(2,128)}, f32[2,4,64,64]{2,0,3,1:T(2,128)S(1)}, u32[]{:S(2)}) copy-start(f32[2,4,64,64]{2,0,3,1:T(2,128)S(1)} %get-tuple-element.1230) | copy-start | bytes 393220 | tf_op jit(solution)/shard_map/while
  153.8 2.5 copy-start.5
  179.8 3.7 %copy-start.11 = (f32[4,256,64]{1,2,0:T(8,128)S(1)}, f32[4,256,64]{1,2,0:T(8,128)}, u32[]{:S(2)}) copy-start(f32[4,256,64]{1,2,0:T(8,128)} %rev.37) | copy-start | bytes 786436
  186.6 36.4 %copy-start.2 = (f32[4,128,64]{1,2,0:T(8,128)S(1)}, f32[4,128,64]{1,2,0:T(8,128)}, u32[]{:S(2)}) copy-start(f32[4,128,64]{1,2,0:T(8,128)} %copy-done.1) | copy-start | bytes 393220
  273.6 36.8 %copy-start.7 = (f32[2,4,64,128]{3,2,0,1:T(8,128)S(1)}, f32[2,4,64,128]{3,2,0,1:T(8,128)}, u32[]{:S(2)}) copy-start(f32[2,4,64,128]{3,2,0,1:T(8,128)} %get-tuple-element.543) | copy-start | bytes 786436
  310.3 4.2 %copy-start.8 = (f32[2,4,64,128]{3,2,0,1:T(8,128)S(1)}, f32[2,4,64,128]{3,2,0,1:T(8,128)}, u32[]{:S(2)}) copy-start(f32[2,4,64,128]{3,2,0,1:T(8,128)} %get-tuple-element.538) | copy-start | bytes 786436
  311.2 4.0 %copy-start.14 = (f32[4,64,64]{2,1,0:T(8,128)S(1)}, f32[4,64,64]{2,1,0:T(8,128)}, u32[]{:S(2)}) copy-start(f32[4,64,64]{2,1,0:T(8,128)} %copy.121) | copy-start | bytes 196612
  313.2 3.0 copy-start.12
  315.5 39.8 %copy-start.10 = (bf16[32,2048]{1,0:T(8,128)(2,1)S(1)}, bf16[32,2048]{1,0:T(8,128)(2,1)}, u32[]{:S(2)}) copy-start(bf16[32,2048]{1,0:T(8,128)(2,1)} %param.28) | copy-start | bytes 393220
Sparse Core Ops, SparseCore 0:
  8.9 29.8 all-gather.7
  40.3 27.9 all-gather.9
  70.0 27.9 all-gather.11
  317.5 37.7 reduce-scatter.1
where the time goes:
time: 366 us; the launch traced here: 363 us
  blocking collectives  122 us (33%)
  matrix products  92.8 us (25%)
  local copies, waits for them, and re-layouts  77.6 us (21%)
  waiting for transfers between devices  44.6 us (12%)
  between operations  13.8 us (4%)
  other arithmetic  9.35 us (3%)
    all_gather x4, blocking collectives, carried_in(): lax.all_gather(part.astype(kind), axis)  45.7 us
    dynamic_slice x68, local copies, waits for them, and re-layouts, run_blocks(): last_state, outputs = lax.scan(advance, memory, stacked)  42.3 us
    reduce_scatter x1, waiting for transfers between devices, shards(): lax.psum_scatter(matmul(normed_rows, w_out).astype(jnp.bfloat16), 'tp', s...  37.9 us
    reshape x18, local copies, waits for them, and re-layouts, split_blocks(): tensor.reshape(head_count, tokens // BLOCK, BLOCK, channels)  21.3 us
    psum x1, blocking collectives, shards(): summed = lax.psum(partial_mod, 'sp')  16.6 us
    dot_general x60, matrix products, unit_lower_inverse(): jnp.einsum('hij,hjk->hik', inverse, identity + squared, precision=EXACT_M...  15.6 us
    dot_general x60, matrix products, unit_lower_inverse(): squared = jnp.einsum('hij,hjk->hik', squared, squared, precision=EXACT_MODE)  15.3 us
    dot_general x15, matrix products, matmul(): return jnp.dot(lhs_matrix, rhs_matrix, preferred_element_type=jnp.float32)  14.7 us
  transfers between devices with their start and end apart: 4, of which 2 were waited for; matrix products, arithmetic and copies ran while one was open for 8% of the time, Pallas kernels for 0%

commit v1 on v0

v1 whole, which is shorter than its diff:
```python
import functools

import jax
import jax.numpy as jnp
from jax import lax
from jax.experimental import pallas as pl
from jax.experimental.pallas import tpu as pltpu
from jax.sharding import PartitionSpec as P

HEAD = 64
BLOCK = 64
NORM_EPS = 1e-06
HEAD_EPS = 0.00064
DECAY_SCALE = 0.6065306597126334
MESH = pl.DeviceIdType.MESH
F32, BF16 = jnp.float32, jnp.bfloat16
NN = (((1,), (0,)), ((), ()))
NT = (((1,), (1,)), ((), ()))
TN = (((0,), (0,)), ((), ()))


def iota(shape, axis):
    return lax.broadcasted_iota(jnp.int32, shape, axis)


def mm(a, b, dims=NN):
    return lax.dot_general(a, b, dims, preferred_element_type=F32)


def split(x):
    high = x.astype(BF16)
    return (high, (x - high.astype(F32)).astype(BF16))


def mm3(a, b, dims=NN):
    return mm(a[0], b[0], dims) + (mm(a[1], b[0], dims) + mm(a[0], b[1], dims))


def mm2(a, b, dims=NN):
    return mm(a[0], b, dims) + mm(a[1], b, dims)


def block_diag(x, wide):
    rows, cols = x.shape
    heads = cols // wide
    shape = (heads * rows, cols)
    mask = (iota(shape, 0) // rows == iota(shape, 1) // wide).astype(F32)
    if rows % 16 == 0:
        return jnp.concatenate([x] * heads, axis=0) * mask.astype(x.dtype)
    return (jnp.concatenate([x.astype(F32)] * heads, axis=0) * mask).astype(x.dtype)


def bd(pair, wide):
    return (block_diag(pair[0], wide), block_diag(pair[1], wide))


def fold(full):
    size = full.shape[0]
    heads = size // HEAD
    kept = jnp.where(iota(full.shape, 0) // HEAD == iota(full.shape, 1) // HEAD, full, 0.0)
    total = kept[:HEAD]
    for h in range(1, heads):
        total = total + kept[h * HEAD : (h + 1) * HEAD]
    return total


def head_sum(x):
    size = x.shape[1]
    ones = (iota((size, size), 0) // HEAD == iota((size, size), 1) // HEAD).astype(F32).astype(BF16)
    return mm2(split(x), ones)


def block_map(key, value, log_decay, beta, kappa, receive, reverse):
    length, cols = key.shape
    heads = cols // HEAD
    row, col = iota((length, length), 0), iota((length, length), 1)
    reach = (col >= row) if reverse else (col <= row)
    reach = reach.astype(F32).astype(BF16)
    parts = split(log_decay)
    cumulative = mm(reach, parts[0]) + mm(reach, parts[1])
    previous = cumulative - log_decay
    mid = length // 2 if reverse else length // 2 - 1
    end = 0 if reverse else length - 1
    centre = cumulative[mid : mid + 1]
    closing = cumulative[end : end + 1]
    inward = jnp.exp(centre - cumulative)
    remain = jnp.exp(closing - cumulative)
    outward = kappa * jnp.exp(previous - centre)
    lhs = outward
    if receive is not None:
        lhs = jnp.concatenate([outward, receive * jnp.exp(cumulative - centre)], axis=0)
    lhs = split(lhs)
    mix_beta = mm3(lhs, bd(split(beta * inward), HEAD), NT)
    mix_key = mm3(lhs, bd(split(key * inward), HEAD), NT)
    shape = (length, heads * length)
    token, source = iota(shape, 0), iota(shape, 1) % length
    strict = (source > token) if reverse else (source < token)
    within = (source >= token) if reverse else (source <= token)
    strictly = jnp.where(strict, mix_beta[:length], 0.0)
    key_mix = jnp.where(strict, mix_key[:length], 0.0)
    eye = (source == token).astype(F32)
    inverse = eye - strictly
    parts = split(strictly)
    square = mm3(parts, bd(parts, length))
    rounds = (length - 1).bit_length() - 1
    for i in range(rounds):
        parts = split(square)
        rhs = bd(parts, length)
        if i == rounds - 1:
            inverse = inverse + mm3(split(inverse), rhs)
        else:
            both = mm3(split(jnp.concatenate([inverse, square], axis=0)), rhs)
            inverse = inverse + both[:length]
            square = both[length:]
    value_bf = value.astype(BF16)
    value_bd = block_diag(value_bf, HEAD)
    pushed = mm2(split(key_mix), value_bd)
    inverse = split(inverse)
    taken = mm3(inverse, bd(split(kappa * jnp.exp(previous)), HEAD))
    removed = mm3(inverse, bd(split(pushed), HEAD))
    beta_rest = split(beta * remain)
    size = (HEAD, cols)
    eye_row = iota(size, 0) == iota(size, 1) % HEAD
    move = jnp.where(eye_row, jnp.exp(closing), 0.0) - fold(mm3(split(taken), beta_rest, TN))
    key_rest = split(key * remain)
    write = mm(value_bf, key_rest[0], TN) + mm(value_bf, key_rest[1], TN)
    write = fold(write - mm3(split(removed), beta_rest, TN))
    if receive is None:
        return (move, write, None, None)
    read_key = split(jnp.where(within, mix_key[length:], 0.0))
    read_beta = split(jnp.where(within, mix_beta[length:], 0.0))
    query = receive * jnp.exp(cumulative) - mm3(read_beta, bd(split(taken), HEAD))
    local = mm2(read_key, value_bd) - mm3(read_beta, bd(split(removed), HEAD))
    return (move, write, query, local)


def step_state(state, move, write):
    return mm2(split(state), block_diag(move.astype(BF16), HEAD)) + write.astype(F32)


def chain_map(first, then):
    return (
        mm3(split(first[0]), bd(split(then[0]), HEAD)),
        mm3(split(first[1]), bd(split(then[0]), HEAD)) + then[1],
    )


def kernel(
    n_sp, n_tp,
    lat_ref, ctx_ref, cond_ref, ctx_cond_ref, w_mod_ref, w_recept_ref, w_key_ref, w_value_ref,
    decay_down_ref, decay_up_ref, decay_base_ref, decay_shift_ref, rate_down_ref, rate_up_ref,
    rate_bias_ref, w_out_ref,
    out_ref,
    mod_parts, mod_sum, mod_full, lat_all, hid, weights, acc, ctx_maps, ctx_own, lat_maps, lat_own,
    state, branch_own, branch_in,
    load_sem, msend, mrecv, gsend, grecv, lsend, lrecv, wsend, wrecv, csend, crecv,
    ssend, srecv, bsend, brecv,
):
    sp, tp = lax.axis_index("sp"), lax.axis_index("tp")
    model = lat_ref.shape[1]
    rows = lat_ref.shape[0]
    slab = w_mod_ref.shape[0]
    mod_cols = w_mod_ref.shape[1]
    cols = w_recept_ref.shape[1]
    tokens = rows * n_tp
    half = slab // 2

    loads = [
        pltpu.make_async_copy(ref, weights.at[sp, i], load_sem.at[i])
        for i, ref in enumerate((w_recept_ref, w_key_ref, w_value_ref))
    ]
    for load in loads:
        load.start()

    barrier = pltpu.get_barrier_semaphore()
    for k in range(1, n_sp):
        pl.semaphore_signal(
            barrier, inc=1, device_id={"sp": lax.rem(sp + k, n_sp)}, device_id_type=MESH
        )
    for k in range(1, n_tp):
        pl.semaphore_signal(
            barrier, inc=1, device_id={"tp": lax.rem(tp + k, n_tp)}, device_id_type=MESH
        )

    here = pl.ds(sp, 1)

    def silu(v):
        return v / (1.0 + jnp.exp(-v))

    activated = jnp.concatenate(
        [silu(cond_ref[here, :]), silu(ctx_cond_ref[here, :])], axis=0
    ).astype(BF16)
    mod_parts[0] = mm(activated, w_mod_ref[...])
    pl.semaphore_wait(barrier, n_sp - 1 + n_tp - 1)

    def remote(src, dst, send, recv, axis, target):
        return pltpu.make_async_remote_copy(
            src_ref=src, dst_ref=dst, send_sem=send, recv_sem=recv,
            device_id={axis: target}, device_id_type=MESH,
        )

    sent = []
    mods = []
    for k in range(1, n_sp):
        copy = remote(
            mod_parts.at[0], mod_parts.at[k], msend.at[k], mrecv.at[k], "sp", lax.rem(sp + k, n_sp)
        )
        copy.start()
        mods.append(copy)
    lats = []
    mine = pl.ds(pl.multiple_of(tp * rows, rows), rows)
    for k in range(1, n_tp):
        copy = remote(
            lat_ref, lat_all.at[mine, :], lsend.at[k], lrecv.at[k], "tp", lax.rem(tp + k, n_tp)
        )
        copy.start()
        lats.append(copy)
    lat_all[mine, :] = lat_ref[...]
    for load in loads:
        load.wait()
    right, left = lax.rem(sp + 1, n_sp), lax.rem(sp + n_sp - 1, n_sp)
    far = n_sp // 2

    def hop(i, direction):
        back = 1 if direction == 0 else -1
        which = lax.rem(sp + n_sp - back * (i - 1), n_sp)
        part = weights.at[which]
        if i == far:
            part = part.at[:, pl.ds(direction * half, half), :]
        return remote(
            part, part, wsend.at[direction, i], wrecv.at[direction, i], "sp",
            right if direction == 0 else left,
        )

    hops = {}
    for direction in range(2):
        hops[1, direction] = hop(1, direction)
        hops[1, direction].start()

    for copy in mods:
        copy.wait_recv()
    total = mod_parts[0]
    for k in range(1, n_sp):
        total = total + mod_parts[k]
    mod_sum[...] = total
    where_cols = pl.ds(pl.multiple_of(tp * mod_cols, mod_cols), mod_cols)
    mod_full[:, where_cols] = total
    gathers = []
    for k in range(1, n_tp):
        copy = remote(
            mod_sum, mod_full.at[:, where_cols], gsend.at[k], grecv.at[k], "tp",
            lax.rem(tp + k, n_tp),
        )
        copy.start()
        gathers.append(copy)
    for copy in lats:
        copy.wait_recv()
    for copy in gathers:
        copy.wait_recv()
    modulation = mod_full[...]

    def modulate(block, r):
        values = block.astype(F32)
        normed = values * lax.rsqrt(jnp.mean(values * values, axis=-1, keepdims=True) + NORM_EPS)
        return (
            normed * (1.0 + modulation[r : r + 1, model : 2 * model])
            + modulation[r : r + 1, :model]
        ).astype(BF16)

    hid[:tokens, :] = modulate(lat_all[...], 0)
    hid[tokens:, :] = modulate(ctx_ref[...], 1)
    hidden = hid[...]
    decay_low = jnp.tanh(mm(hidden, decay_down_ref[...]).astype(BF16).astype(F32)).astype(BF16)
    rate_low = mm(hidden, rate_down_ref[...]).astype(BF16)
    pre = decay_base_ref[...] + mm(decay_low, decay_up_ref[...])
    rate = 1.0 / (1.0 + jnp.exp(-(rate_bias_ref[...] + mm(rate_low, rate_up_ref[...]))))

    def add_slab(which, first=False):
        lanes = pl.ds(pl.multiple_of(which * slab, slab), slab) if slab % 128 == 0 else None
        if lanes is None:
            return
        piece = hid[:, lanes]
        for m in range(3):
            product = mm(piece, weights[which, m])
            acc[m] = product if first else acc[m] + product

    by_slab = slab % 128 == 0
    if by_slab:
        add_slab(sp, True)
    for i in range(1, far + 1):
        for direction in range(2):
            hops[i, direction].wait_recv()
        if i < far:
            for direction in range(2):
                hops[i + 1, direction] = hop(i + 1, direction)
                hops[i + 1, direction].start()
        if by_slab:
            add_slab(lax.rem(sp + n_sp - i, n_sp))
            if i < far:
                add_slab(lax.rem(sp + i, n_sp))
    if not by_slab:
        for m in range(3):
            joined = jnp.concatenate([weights[j, m] for j in range(n_sp)], axis=0)
            acc[m] = mm(hidden, joined)

    receive = acc[0].astype(BF16).astype(F32)
    key = acc[1].astype(BF16).astype(F32)
    value = acc[2].astype(BF16).astype(F32)
    kappa = key * lax.rsqrt(head_sum(key * key) + NORM_EPS)
    beta = kappa * rate
    lane_head = iota((tokens, cols), 1) // HEAD
    shift = jnp.zeros((tokens, cols), F32)
    for h in range(cols // HEAD):
        shift = jnp.where(lane_head == h, decay_shift_ref[:, h : h + 1], shift)
    pre = jnp.concatenate([pre[:tokens] + shift, pre[tokens:]], axis=0)
    log_decay = -DECAY_SCALE / (1.0 + jnp.exp(-pre))

    def blocks(start, stop, reverse, with_read):
        found = []
        length = min(BLOCK, stop - start)
        for low in range(start, stop, length):
            at = slice(low, low + length)
            found.append(
                block_map(
                    key[at], value[at], log_decay[at], beta[at], kappa[at],
                    receive[at] if with_read else None, reverse,
                )
            )
        return found

    def joined(found, reverse):
        order = found[::-1] if reverse else found
        result = (order[0][0], order[0][1])
        for one in order[1:]:
            result = chain_map(result, (one[0], one[1]))
        return result

    ctx_end = hid.shape[0]
    for d in range(2):
        move, write = joined(blocks(tokens, ctx_end, d == 1, False), d == 1)
        ctx_own[d, :HEAD] = move.astype(BF16)
        ctx_own[d, HEAD:] = write.astype(BF16)
    ctxs = []
    for k in range(1, n_sp):
        copy = remote(
            ctx_own, ctx_maps.at[sp], csend.at[k], crecv.at[k], "sp", lax.rem(sp + k, n_sp)
        )
        copy.start()
        ctxs.append(copy)
    ctx_maps[sp] = ctx_own[...]

    founds = []
    for d in range(2):
        found = blocks(0, tokens, d == 1, True)
        founds.append(found)
        move, write = joined(found, d == 1)
        lat_own[d, :HEAD] = move.astype(BF16)
        lat_own[d, HEAD:] = write.astype(BF16)

    def lat_copy(k, d):
        target = sp + k if d == 0 else sp - k
        return remote(
            lat_own.at[d], lat_maps.at[d, sp], ssend.at[d, k], srecv.at[d, k], "sp", target
        )

    for k in range(1, n_sp):

        @pl.when(sp + k < n_sp)
        def _():
            lat_copy(k, 0).start()

        @pl.when(sp - k >= 0)
        def _():
            lat_copy(k, 1).start()

    for copy in ctxs:
        copy.wait_recv()
    fwd = ctx_maps[0, 0, HEAD:].astype(F32)
    bwd = ctx_maps[n_sp - 1, 1, HEAD:].astype(F32)
    for j in range(1, n_sp):
        fwd = step_state(fwd, ctx_maps[j, 0, :HEAD], ctx_maps[j, 0, HEAD:])
        at = n_sp - 1 - j
        bwd = step_state(bwd, ctx_maps[at, 1, :HEAD], ctx_maps[at, 1, HEAD:])
    state[0] = fwd
    state[1] = bwd
    for k in range(n_sp - 1, 0, -1):

        @pl.when(sp - k >= 0)
        def _():
            remote(
                lat_own.at[0], lat_maps.at[0, sp - k], ssend.at[0, k], srecv.at[0, k], "sp", sp - k
            ).wait_recv()
            state[0] = step_state(
                state[0], lat_maps[0, sp - k, :HEAD], lat_maps[0, sp - k, HEAD:]
            )

        @pl.when(sp + k < n_sp)
        def _():
            remote(
                lat_own.at[1], lat_maps.at[1, sp + k], ssend.at[1, k], srecv.at[1, k], "sp", sp + k
            ).wait_recv()
            state[1] = step_state(
                state[1], lat_maps[1, sp + k, :HEAD], lat_maps[1, sp + k, HEAD:]
            )

    outputs = []
    for d in range(2):
        entering = state[d]
        found = founds[d]
        order = list(range(len(found)))
        if d == 1:
            order = order[::-1]
        got = [None] * len(found)
        for n, b in enumerate(order):
            move, write, query, local = found[b]
            got[b] = mm3(split(query), bd(split(entering), HEAD), NT) + local
            if n + 1 < len(order):
                entering = mm3(split(entering), bd(split(move), HEAD)) + write
        outputs.append(jnp.concatenate(got, axis=0))
    mixed = outputs[0] + outputs[1]
    centred = mixed - head_sum(mixed) * (1.0 / HEAD)
    variance = head_sum(centred * centred) * (1.0 / HEAD)
    normed = (centred * lax.rsqrt(variance + HEAD_EPS)).astype(BF16)
    product = mm(normed, w_out_ref[...]).astype(BF16)
    for t in range(n_tp):
        branch_own[t] = product[t * rows : (t + 1) * rows]
    backs = []
    for k in range(1, n_tp):
        target = lax.rem(tp + k, n_tp)
        copy = remote(
            branch_own.at[target], branch_in.at[k], bsend.at[k], brecv.at[k], "tp", target
        )
        copy.start()
        backs.append(copy)
    branch = branch_own[tp].astype(F32)
    for k, copy in enumerate(backs, 1):
        copy.wait_recv()
        branch = branch + branch_in[k].astype(F32)
    branch = branch.astype(BF16).astype(F32)
    gate = modulation[0:1, 2 * model :]
    out_ref[...] = (lat_ref[...].astype(F32) + gate * branch).astype(BF16)

    for copy in mods + lats + gathers + ctxs + backs + list(hops.values()):
        copy.wait_send()
    for k in range(1, n_sp):

        @pl.when(sp + k < n_sp)
        def _():
            lat_copy(k, 0).wait_send()

        @pl.when(sp - k >= 0)
        def _():
            lat_copy(k, 1).wait_send()


def shards(
    latent, context, condition, ctx_condition, w_mod, w_recept, w_key, w_value, w_decay_down,
    w_decay_up, decay_base, decay_shift, w_rate_down, w_rate_up, rate_bias, w_out,
):
    n_sp, n_tp = lax.axis_size("sp"), lax.axis_size("tp")
    rows, model = latent.shape
    slab, mod_cols = w_mod.shape
    cols = w_recept.shape[1]
    tokens = rows * n_tp
    every = tokens + context.shape[0]
    dma = pltpu.SemaphoreType.DMA
    vmem = pl.BlockSpec(memory_space=pltpu.VMEM)
    hbm = pl.BlockSpec(memory_space=pl.ANY)
    return pl.pallas_call(
        functools.partial(kernel, n_sp, n_tp),
        out_shape=jax.ShapeDtypeStruct((rows, model), BF16),
        in_specs=[vmem] * 5 + [hbm] * 3 + [vmem] * 8,
        out_specs=vmem,
        scratch_shapes=[
            pltpu.VMEM((n_sp, 2, mod_cols), F32),
            pltpu.VMEM((2, mod_cols), F32),
            pltpu.VMEM((2, mod_cols * n_tp), F32),
            pltpu.VMEM((tokens, model), BF16),
            pltpu.VMEM((every, model), BF16),
            pltpu.VMEM((n_sp, 3, slab, cols), BF16),
            pltpu.VMEM((3, every, cols), F32),
            pltpu.VMEM((n_sp, 2, 2 * HEAD, cols), BF16),
            pltpu.VMEM((2, 2 * HEAD, cols), BF16),
            pltpu.VMEM((2, n_sp, 2 * HEAD, cols), BF16),
            pltpu.VMEM((2, 2 * HEAD, cols), BF16),
            pltpu.VMEM((2, HEAD, cols), F32),
            pltpu.VMEM((n_tp, rows, model), BF16),
            pltpu.VMEM((n_tp, rows, model), BF16),
            dma((3,)),
            dma((n_sp,)), dma((n_sp,)),
            dma((n_tp,)), dma((n_tp,)),
            dma((n_tp,)), dma((n_tp,)),
            dma((2, n_sp // 2 + 1)), dma((2, n_sp // 2 + 1)),
            dma((n_sp,)), dma((n_sp,)),
            dma((2, n_sp)), dma((2, n_sp)),
            dma((n_tp,)), dma((n_tp,)),
        ],
        compiler_params=pltpu.CompilerParams(collective_id=0, has_side_effects=True),
    )(
        latent, context, condition.reshape(n_sp, slab),
        ctx_condition.reshape(n_sp, slab), w_mod, w_recept, w_key, w_value,
        w_decay_down, w_decay_up, decay_base[None], decay_shift, w_rate_down, w_rate_up,
        rate_bias[None], w_out,
    )


def solution(mesh):
    return jax.shard_map(
        shards,
        mesh=mesh,
        in_specs=(
            P(("grp", "sp", "tp"), None),
            P(("grp", "sp"), None),
            P("grp"),
            P(),
            P("sp", "tp"),
            P("sp", "tp"),
            P("sp", "tp"),
            P("sp", "tp"),
            P(),
            P(None, "tp"),
            P("tp"),
            P(("grp", "sp"), "tp"),
            P(),
            P(None, "tp"),
            P("tp"),
            P("tp", None),
        ),
        out_specs=P(("grp", "sp", "tp"), None),
        check_vma=False,
    )
```

time: 366 us -> 109 us (0.30)
  blocking collectives: 122 us -> 0 us
  Pallas kernels: 0 us -> 99.6 us
  matrix products: 92.8 us -> 0 us
  local copies, waits for them, and re-layouts: 77.6 us -> 9.49 us
  waiting for transfers between devices: 44.6 us -> 0 us
  between operations: 13.8 us -> 0.01 us
  other arithmetic: 9.35 us -> 0 us
    all_gather x10 -> x0, blocking collectives: 105 us -> none  [the longest x4 45.7 us: carried_in(): lax.all_gather(part.astype(kind), axis)]
    pallas_call x0 -> x1, Pallas kernels: none -> 99.6 us  [shards(): pl.pallas_call(functools.partial(kernel, n_sp, n_tp), out_shape=jax.Shape...]
    dot_general x259 -> x0, matrix products: 92.8 us -> none  [the longest x60 15.6 us: unit_lower_inverse(): jnp.einsum('hij,hjk->hik', inverse, identity + squared, precision=EXACT_M...]
    dynamic_slice x84 -> x0, local copies, waits for them, and re-layouts: 43.2 us -> none  [the longest x68 42.3 us: run_blocks(): last_state, outputs = lax.scan(advance, memory, stacked)]
    reduce_scatter x1 -> x0, waiting for transfers between devices: 37.9 us -> none  [shards(): lax.psum_scatter(matmul(normed_rows, w_out).astype(jnp.bfloat16), 'tp', s...]
    reshape x18 -> x2, local copies, waits for them, and re-layouts: 21.3 us -> 2.59 us  [the longest x1 1.3 us: shards(): ctx_condition.reshape(n_sp, slab)]
    psum x1 -> x0, blocking collectives: 16.6 us -> none  [shards(): summed = lax.psum(partial_mod, 'sp')]
    unnamed x40 -> x4, local copies, waits for them, and re-layouts: 0.31 us -> 6.9 us
  transfers between devices with their start and end apart: 4 -> 0, of which waited for: 2 -> 0; matrix products, arithmetic and copies ran while one was open for 8% -> 0% of each run, Pallas kernels for 0% -> 0%
where the time goes in v1:
time: 109 us
  Pallas kernels  99.6 us (91%)
  local copies, waits for them, and re-layouts  9.49 us (9%)
    pallas_call x1, Pallas kernels, shards(): pl.pallas_call(functools.partial(kernel, n_sp, n_tp), out_shape=jax.Shape...  99.6 us
    unnamed x4, local copies, waits for them, and re-layouts  6.9 us

profile of v1, /device:TPU:1, one launch (start us, length us, event | category | flops | bytes accessed | tf_op | source)
XLA Modules:
  0.0 109.1 jit_solution(8051410677997906510)
XLA Ops:
  0.0 1.3 %reshape.6.cond_ref = f32[4,512]{1,0:T(4,128)} reshape(f32[2048]{0:T(1024)} %param.18) | data formatting | bytes 16384 | tf_op jit(solution)/shard_map/reshape | solution.py:500
  1.3 1.3 %reshape.7.ctx_cond_ref = f32[4,512]{1,0:T(4,128)} reshape(f32[2048]{0:T(1024)} %param.19) | data formatting | bytes 16384 | tf_op jit(solution)/shard_map/reshape | solution.py:501
  2.6 1.4 %copy.18.decay_shift_ref = f32[128,4]{1,0:T(8,128)} copy(f32[128,4]{0,1:T(4,128)} %param.27) | data formatting | bytes 4096 | tf_op args[11]
  4.0 1.9 %copy.17.decay_down_ref = bf16[2048,64]{1,0:T(8,128)(2,1)} copy(bf16[2048,64]{0,1:T(8,128)(2,1)} %param.24) | data formatting | bytes 524288 | tf_op args[8]
  6.0 2.0 %copy.19.rate_down_ref = bf16[2048,64]{1,0:T(8,128)(2,1)} copy(bf16[2048,64]{0,1:T(8,128)(2,1)} %param.28) | data formatting | bytes 524288 | tf_op args[12]
  7.9 99.6 %shard_map.154 = bf16[32,2048]{1,0:T(8,128)(2,1)} custom-call(bf16[32,2048]{1,0:T(8,128)(2,1)} %lat_ref.1, bf16[64,2048]{1,0:T(8,128)(2,1)} %ctx_ref.1, f32[4,512]{1,0:T(4,128)} %reshape.6.cond_ref, f32[4,512]{1,0:T(4,128)} %reshape.7.ctx_cond_ref, bf16[512,1536]{1,0:T(8,128)(2,1)} %w_mod_ref.1, bf16[512,256]{1,0:T(8,128)(2,1)} %w_recept_ref.1, ...), custom_call_target="tpu_custom_call" | custom-call | tf_op jit(solution)/shard_map/pallas_call | solution.py:469
  107.5 1.6 %copy.21 = bf16[32,2048]{1,0:T(8,128)(2,1)} copy(bf16[32,2048]{1,0:T(8,128)(2,1)} %shard_map.154) | data formatting | bytes 262144

commit v2 on v1

--- a/solution.py
+++ b/solution.py
@@ -70,7 +70,22 @@
     return mm2(split(x), ones)
 
 
-def block_map(key, value, log_decay, beta, kappa, receive, reverse):
+def lockstep(runs):
+    results = [None] * len(runs)
+    live = list(range(len(runs)))
+    while live:
+        still = []
+        for i in live:
+            try:
+                next(runs[i])
+                still.append(i)
+            except StopIteration as end:
+                results[i] = end.value
+        live = still
+    return results
+
+
+def block_map(key, value, log_decay, beta, kappa, reverse):
     length, cols = key.shape
     heads = cols // HEAD
     row, col = iota((length, length), 0), iota((length, length), 1)
@@ -78,6 +93,7 @@
     reach = reach.astype(F32).astype(BF16)
     parts = split(log_decay)
     cumulative = mm(reach, parts[0]) + mm(reach, parts[1])
+    yield
     previous = cumulative - log_decay
     mid = length // 2 if reverse else length // 2 - 1
     end = 0 if reverse else length - 1
@@ -85,23 +101,26 @@
     closing = cumulative[end : end + 1]
     inward = jnp.exp(centre - cumulative)
     remain = jnp.exp(closing - cumulative)
-    outward = kappa * jnp.exp(previous - centre)
-    lhs = outward
-    if receive is not None:
-        lhs = jnp.concatenate([outward, receive * jnp.exp(cumulative - centre)], axis=0)
-    lhs = split(lhs)
-    mix_beta = mm3(lhs, bd(split(beta * inward), HEAD), NT)
-    mix_key = mm3(lhs, bd(split(key * inward), HEAD), NT)
+    outward = split(kappa * jnp.exp(previous - centre))
+    beta_in = bd(split(beta * inward), HEAD)
+    key_in = bd(split(key * inward), HEAD)
+    yield
+    mix_beta = mm3(outward, beta_in, NT)
+    mix_key = mm3(outward, key_in, NT)
+    yield
     shape = (length, heads * length)
     token, source = iota(shape, 0), iota(shape, 1) % length
     strict = (source > token) if reverse else (source < token)
     within = (source >= token) if reverse else (source <= token)
-    strictly = jnp.where(strict, mix_beta[:length], 0.0)
-    key_mix = jnp.where(strict, mix_key[:length], 0.0)
-    eye = (source == token).astype(F32)
-    inverse = eye - strictly
+    strictly = jnp.where(strict, mix_beta, 0.0)
+    key_mix = jnp.where(strict, mix_key, 0.0)
+    inverse = (source == token).astype(F32) - strictly
     parts = split(strictly)
     square = mm3(parts, bd(parts, length))
+    value_bf = value.astype(BF16)
+    value_bd = block_diag(value_bf, HEAD)
+    pushed = mm2(split(key_mix), value_bd)
+    yield
     rounds = (length - 1).bit_length() - 1
     for i in range(rounds):
         parts = split(square)
@@ -112,26 +131,33 @@
             both = mm3(split(jnp.concatenate([inverse, square], axis=0)), rhs)
             inverse = inverse + both[:length]
             square = both[length:]
-    value_bf = value.astype(BF16)
-    value_bd = block_diag(value_bf, HEAD)
-    pushed = mm2(split(key_mix), value_bd)
+        yield
     inverse = split(inverse)
     taken = mm3(inverse, bd(split(kappa * jnp.exp(previous)), HEAD))
     removed = mm3(inverse, bd(split(pushed), HEAD))
+    yield
+    taken, removed = split(taken), split(removed)
     beta_rest = split(beta * remain)
+    key_rest = split(key * remain)
     size = (HEAD, cols)
     eye_row = iota(size, 0) == iota(size, 1) % HEAD
-    move = jnp.where(eye_row, jnp.exp(closing), 0.0) - fold(mm3(split(taken), beta_rest, TN))
-    key_rest = split(key * remain)
+    move = jnp.where(eye_row, jnp.exp(closing), 0.0) - fold(mm3(taken, beta_rest, TN))
     write = mm(value_bf, key_rest[0], TN) + mm(value_bf, key_rest[1], TN)
-    write = fold(write - mm3(split(removed), beta_rest, TN))
-    if receive is None:
-        return (move, write, None, None)
-    read_key = split(jnp.where(within, mix_key[length:], 0.0))
-    read_beta = split(jnp.where(within, mix_beta[length:], 0.0))
-    query = receive * jnp.exp(cumulative) - mm3(read_beta, bd(split(taken), HEAD))
-    local = mm2(read_key, value_bd) - mm3(read_beta, bd(split(removed), HEAD))
-    return (move, write, query, local)
+    write = fold(write - mm3(removed, beta_rest, TN))
+    return (move, write, (cumulative, centre, within, beta_in, key_in, value_bd, taken, removed))
+
+
+def block_read(receive, kept):
+    cumulative, centre, within, beta_in, key_in, value_bd, taken, removed = kept
+    reading = split(receive * jnp.exp(cumulative - centre))
+    read_beta = mm3(reading, beta_in, NT)
+    read_key = mm3(reading, key_in, NT)
+    yield
+    read_key = split(jnp.where(within, read_key, 0.0))
+    read_beta = split(jnp.where(within, read_beta, 0.0))
+    query = receive * jnp.exp(cumulative) - mm3(read_beta, bd(taken, HEAD))
+    local = mm2(read_key, value_bd) - mm3(read_beta, bd(removed, HEAD))
+    return (query, local)
 
 
 def step_state(state, move, write):
@@ -151,9 +177,9 @@
     decay_down_ref, decay_up_ref, decay_base_ref, decay_shift_ref, rate_down_ref, rate_up_ref,
     rate_bias_ref, w_out_ref,
     out_ref,
-    mod_parts, mod_sum, mod_full, lat_all, hid, weights, acc, ctx_maps, ctx_own, lat_maps, lat_own,
+    mod_parts, mod_sum, mod_full, lat_all, hid, weights, ctx_maps, ctx_own, lat_maps, lat_own,
     state, branch_own, branch_in,
-    load_sem, msend, mrecv, gsend, grecv, lsend, lrecv, wsend, wrecv, csend, crecv,
+    load_sem, msend, mrecv, gsend, grecv, lsend, lrecv, wsend, wrecv, ysend, yrecv, csend, crecv,
     ssend, srecv, bsend, brecv,
 ):
     sp, tp = lax.axis_index("sp"), lax.axis_index("tp")
@@ -165,9 +191,14 @@
     tokens = rows * n_tp
     half = slab // 2
 
+    grp = lax.axis_index("grp")
     loads = [
-        pltpu.make_async_copy(ref, weights.at[sp, i], load_sem.at[i])
-        for i, ref in enumerate((w_recept_ref, w_key_ref, w_value_ref))
+        pltpu.make_async_copy(
+            ref,
+            weights.at[m, pl.ds(pl.multiple_of(sp * slab, slab), slab), :],
+            load_sem.at[m],
+        )
+        for m, ref in enumerate((w_key_ref, w_value_ref, w_recept_ref))
     ]
     for load in loads:
         load.start()
@@ -182,16 +213,21 @@
             barrier, inc=1, device_id={"tp": lax.rem(tp + k, n_tp)}, device_id_type=MESH
         )
 
-    here = pl.ds(sp, 1)
+    pl.semaphore_signal(barrier, inc=1, device_id={"grp": 1 - grp}, device_id_type=MESH)
+
+    if slab % 128 == 0:
+        here = (slice(None), pl.ds(pl.multiple_of(sp * slab, slab), slab))
+    else:
+        here = (pl.ds(sp, 1), slice(None))
 
     def silu(v):
         return v / (1.0 + jnp.exp(-v))
 
     activated = jnp.concatenate(
-        [silu(cond_ref[here, :]), silu(ctx_cond_ref[here, :])], axis=0
+        [silu(cond_ref[here]), silu(ctx_cond_ref[here])], axis=0
     ).astype(BF16)
     mod_parts[0] = mm(activated, w_mod_ref[...])
-    pl.semaphore_wait(barrier, n_sp - 1 + n_tp - 1)
+    pl.semaphore_wait(barrier, n_sp - 1 + n_tp - 1 + 1)
 
     def remote(src, dst, send, recv, axis, target):
         return pltpu.make_async_remote_copy(
@@ -218,24 +254,67 @@
     lat_all[mine, :] = lat_ref[...]
     for load in loads:
         load.wait()
-    right, left = lax.rem(sp + 1, n_sp), lax.rem(sp + n_sp - 1, n_sp)
-    far = n_sp // 2
-
-    def hop(i, direction):
-        back = 1 if direction == 0 else -1
-        which = lax.rem(sp + n_sp - back * (i - 1), n_sp)
-        part = weights.at[which]
-        if i == far:
-            part = part.at[:, pl.ds(direction * half, half), :]
+
+    def piece(m, which, part):
+        start = pl.multiple_of(which * slab + part * half, half)
+        return weights.at[m, pl.ds(start, half), :]
+
+    def hop(m, i, d):
+        which = sp - (i - 1) if d == 0 else sp + (i - 1)
+        part = piece(m, which, grp)
         return remote(
-            part, part, wsend.at[direction, i], wrecv.at[direction, i], "sp",
-            right if direction == 0 else left,
-        )
-
-    hops = {}
-    for direction in range(2):
-        hops[1, direction] = hop(1, direction)
-        hops[1, direction].start()
+            part, part, wsend.at[m, d, i], wrecv.at[m, d, i], "sp", sp + 1 if d == 0 else sp - 1
+        )
+
+    def across(m, i, d):
+        part = piece(m, sp - i if d == 0 else sp + i, grp)
+        return remote(part, part, ysend.at[m, d, i], yrecv.at[m, d, i], "grp", 1 - grp)
+
+    def crossed(m, i, d):
+        part = piece(m, sp - i if d == 0 else sp + i, 1 - grp)
+        return remote(part, part, ysend.at[m, d, i], yrecv.at[m, d, i], "grp", 1 - grp)
+
+    def ahead(d):
+        return sp + 1 < n_sp if d == 0 else sp >= 1
+
+    def behind(i, d):
+        return sp >= i if d == 0 else sp + i < n_sp
+
+    for m in range(3):
+        for d in range(2):
+            pl.when(ahead(d))(lambda m=m, d=d: hop(m, 1, d).start())
+
+    def relay(m, i):
+        for d in range(2):
+
+            @pl.when(behind(i, d))
+            def _(d=d):
+                came = piece(m, sp - i if d == 0 else sp + i, grp)
+                remote(
+                    came, came, wsend.at[m, d, i], wrecv.at[m, d, i], "sp",
+                    sp + 1 if d == 0 else sp - 1,
+                ).wait_recv()
+
+                @pl.when(ahead(d))
+                def _():
+                    hop(m, i + 1, d).start()
+
+                across(m, i, d).start()
+
+    def relay_rest(m, first):
+        def body(i, carry):
+            relay(m, i)
+            return carry
+
+        lax.fori_loop(first, n_sp, body, 0)
+
+    def arrive(m):
+        def body(i, carry):
+            for d in range(2):
+                pl.when(behind(i, d))(lambda d=d: crossed(m, i, d).wait_recv())
+            return carry
+
+        lax.fori_loop(1, n_sp, body, 0)
 
     for copy in mods:
         copy.wait_recv()
@@ -253,6 +332,7 @@
         )
         copy.start()
         gathers.append(copy)
+    relay(0, 1)
     for copy in lats:
         copy.wait_recv()
     for copy in gathers:
@@ -268,65 +348,46 @@
         ).astype(BF16)
 
     hid[:tokens, :] = modulate(lat_all[...], 0)
+    if n_sp > 2:
+        relay(0, 2)
     hid[tokens:, :] = modulate(ctx_ref[...], 1)
     hidden = hid[...]
-    decay_low = jnp.tanh(mm(hidden, decay_down_ref[...]).astype(BF16).astype(F32)).astype(BF16)
-    rate_low = mm(hidden, rate_down_ref[...]).astype(BF16)
+    decay_low = jnp.tanh(mm(hidden, decay_down_ref[...], NT).astype(BF16).astype(F32)).astype(BF16)
+    rate_low = mm(hidden, rate_down_ref[...], NT).astype(BF16)
     pre = decay_base_ref[...] + mm(decay_low, decay_up_ref[...])
     rate = 1.0 / (1.0 + jnp.exp(-(rate_bias_ref[...] + mm(rate_low, rate_up_ref[...]))))
 
-    def add_slab(which, first=False):
-        lanes = pl.ds(pl.multiple_of(which * slab, slab), slab) if slab % 128 == 0 else None
-        if lanes is None:
-            return
-        piece = hid[:, lanes]
-        for m in range(3):
-            product = mm(piece, weights[which, m])
-            acc[m] = product if first else acc[m] + product
-
-    by_slab = slab % 128 == 0
-    if by_slab:
-        add_slab(sp, True)
-    for i in range(1, far + 1):
-        for direction in range(2):
-            hops[i, direction].wait_recv()
-        if i < far:
-            for direction in range(2):
-                hops[i + 1, direction] = hop(i + 1, direction)
-                hops[i + 1, direction].start()
-        if by_slab:
-            add_slab(lax.rem(sp + n_sp - i, n_sp))
-            if i < far:
-                add_slab(lax.rem(sp + i, n_sp))
-    if not by_slab:
-        for m in range(3):
-            joined = jnp.concatenate([weights[j, m] for j in range(n_sp)], axis=0)
-            acc[m] = mm(hidden, joined)
-
-    receive = acc[0].astype(BF16).astype(F32)
-    key = acc[1].astype(BF16).astype(F32)
-    value = acc[2].astype(BF16).astype(F32)
+    relay_rest(0, 3)
+    relay_rest(1, 1)
+    arrive(0)
+    key = mm(hidden, weights[0]).astype(BF16).astype(F32)
+    relay_rest(2, 1)
+    arrive(1)
+    value = mm(hidden, weights[1]).astype(BF16).astype(F32)
     kappa = key * lax.rsqrt(head_sum(key * key) + NORM_EPS)
     beta = kappa * rate
     lane_head = iota((tokens, cols), 1) // HEAD
     shift = jnp.zeros((tokens, cols), F32)
-    for h in range(cols // HEAD):
-        shift = jnp.where(lane_head == h, decay_shift_ref[:, h : h + 1], shift)
+    heads = cols // HEAD
+    padded = jnp.concatenate(
+        [decay_shift_ref[...], jnp.zeros(((-heads) % 8, tokens), F32)], axis=0
+    )
+    by_token = padded.T
+    for h in range(heads):
+        shift = jnp.where(lane_head == h, by_token[:, h : h + 1], shift)
     pre = jnp.concatenate([pre[:tokens] + shift, pre[tokens:]], axis=0)
     log_decay = -DECAY_SCALE / (1.0 + jnp.exp(-pre))
 
-    def blocks(start, stop, reverse, with_read):
-        found = []
+    def blocks(start, stop, reverse):
         length = min(BLOCK, stop - start)
-        for low in range(start, stop, length):
-            at = slice(low, low + length)
-            found.append(
-                block_map(
-                    key[at], value[at], log_decay[at], beta[at], kappa[at],
-                    receive[at] if with_read else None, reverse,
-                )
+        return [
+            block_map(
+                key[low : low + length], value[low : low + length],
+                log_decay[low : low + length], beta[low : low + length],
+                kappa[low : low + length], reverse,
             )
-        return found
+            for low in range(start, stop, length)
+        ]
 
     def joined(found, reverse):
         order = found[::-1] if reverse else found
@@ -336,8 +397,10 @@
         return result
 
     ctx_end = hid.shape[0]
+    found = lockstep(blocks(tokens, ctx_end, False) + blocks(tokens, ctx_end, True))
+    count = len(found) // 2
     for d in range(2):
-        move, write = joined(blocks(tokens, ctx_end, d == 1, False), d == 1)
+        move, write = joined(found[d * count : (d + 1) * count], d == 1)
         ctx_own[d, :HEAD] = move.astype(BF16)
         ctx_own[d, HEAD:] = write.astype(BF16)
     ctxs = []
@@ -349,11 +412,11 @@
         ctxs.append(copy)
     ctx_maps[sp] = ctx_own[...]
 
-    founds = []
+    found = lockstep(blocks(0, tokens, False) + blocks(0, tokens, True))
+    count = len(found) // 2
+    founds = [found[:count], found[count:]]
     for d in range(2):
-        found = blocks(0, tokens, d == 1, True)
-        founds.append(found)
-        move, write = joined(found, d == 1)
+        move, write = joined(founds[d], d == 1)
         lat_own[d, :HEAD] = move.astype(BF16)
         lat_own[d, HEAD:] = write.astype(BF16)
 
@@ -373,6 +436,16 @@
         def _():
             lat_copy(k, 1).start()
 
+    arrive(2)
+    receive = mm(hidden[:tokens], weights[2]).astype(BF16).astype(F32)
+    length = tokens // count
+    reads = lockstep(
+        [
+            block_read(receive[b * length : (b + 1) * length], founds[d][b][2])
+            for d in range(2)
+            for b in range(count)
+        ]
+    )
     for copy in ctxs:
         copy.wait_recv()
     fwd = ctx_maps[0, 0, HEAD:].astype(F32)
@@ -412,7 +485,8 @@
             order = order[::-1]
         got = [None] * len(found)
         for n, b in enumerate(order):
-            move, write, query, local = found[b]
+            move, write, _ = found[b]
+            query, local = reads[d * count + b]
             got[b] = mm3(split(query), bd(split(entering), HEAD), NT) + local
             if n + 1 < len(order):
                 entering = mm3(split(entering), bd(split(move), HEAD)) + write
@@ -440,7 +514,7 @@
     gate = modulation[0:1, 2 * model :]
     out_ref[...] = (lat_ref[...].astype(F32) + gate * branch).astype(BF16)
 
-    for copy in mods + lats + gathers + ctxs + backs + list(hops.values()):
+    for copy in mods + lats + gathers + ctxs + backs:
         copy.wait_send()
     for k in range(1, n_sp):
 
@@ -451,6 +525,15 @@
         @pl.when(sp - k >= 0)
         def _():
             lat_copy(k, 1).wait_send()
+
+    def drain(i, carry):
+        for m in range(3):
+            for d in range(2):
+                pl.when(behind(i - 1, d) & ahead(d))(lambda m=m, d=d: hop(m, i, d).wait_send())
+                pl.when(behind(i, d))(lambda m=m, d=d: across(m, i, d).wait_send())
+        return carry
+
+    lax.fori_loop(1, n_sp, drain, 0)
 
 
 def shards(
@@ -463,6 +546,7 @@
     cols = w_recept.shape[1]
     tokens = rows * n_tp
     every = tokens + context.shape[0]
+    by_row = (1, model) if slab % 128 == 0 else (n_sp, slab)
     dma = pltpu.SemaphoreType.DMA
     vmem = pl.BlockSpec(memory_space=pltpu.VMEM)
     hbm = pl.BlockSpec(memory_space=pl.ANY)
@@ -477,8 +561,7 @@
             pltpu.VMEM((2, mod_cols * n_tp), F32),
             pltpu.VMEM((tokens, model), BF16),
             pltpu.VMEM((every, model), BF16),
-            pltpu.VMEM((n_sp, 3, slab, cols), BF16),
-            pltpu.VMEM((3, every, cols), F32),
+            pltpu.VMEM((3, n_sp * slab, cols), BF16),
             pltpu.VMEM((n_sp, 2, 2 * HEAD, cols), BF16),
             pltpu.VMEM((2, 2 * HEAD, cols), BF16),
             pltpu.VMEM((2, n_sp, 2 * HEAD, cols), BF16),
@@ -490,16 +573,16 @@
             dma((n_sp,)), dma((n_sp,)),
             dma((n_tp,)), dma((n_tp,)),
             dma((n_tp,)), dma((n_tp,)),
-            dma((2, n_sp // 2 + 1)), dma((2, n_sp // 2 + 1)),
+            dma((3, 2, n_sp)), dma((3, 2, n_sp)), dma((3, 2, n_sp)), dma((3, 2, n_sp)),
             dma((n_sp,)), dma((n_sp,)),
             dma((2, n_sp)), dma((2, n_sp)),
             dma((n_tp,)), dma((n_tp,)),
         ],
         compiler_params=pltpu.CompilerParams(collective_id=0, has_side_effects=True),
     )(
-        latent, context, condition.reshape(n_sp, slab),
-        ctx_condition.reshape(n_sp, slab), w_mod, w_recept, w_key, w_value,
-        w_decay_down, w_decay_up, decay_base[None], decay_shift, w_rate_down, w_rate_up,
+        latent, context, condition.reshape(by_row),
+        ctx_condition.reshape(by_row), w_mod, w_recept, w_key, w_value,
+        w_decay_down.T, w_decay_up, decay_base[None], decay_shift.T, w_rate_down.T, w_rate_up,
         rate_bias[None], w_out,
     )
 

time: 109 us -> 69.5 us (0.64)
  Pallas kernels: 99.6 us -> 67.8 us
  local copies, waits for them, and re-layouts: 9.49 us -> 1.57 us
    pallas_call x1, Pallas kernels: 99.6 us -> 67.8 us  [shards(): pl.pallas_call(functools.partial(kernel, n_sp, n_tp), out_shape=jax.Shape...]
    unnamed x4 -> x1, local copies, waits for them, and re-layouts: 6.9 us -> 1.57 us
    reshape x2 -> x0, local copies, waits for them, and re-layouts: 2.59 us -> none  [the longest x1 1.3 us: shards(): ctx_condition.reshape(n_sp, slab)]
where the time goes in v2:
time: 69.5 us; the launch traced here: 69.3 us
  Pallas kernels  67.8 us (98%)
  local copies, waits for them, and re-layouts  1.57 us (2%)
    pallas_call x1, Pallas kernels, shards(): pl.pallas_call(functools.partial(kernel, n_sp, n_tp), out_shape=jax.Shape...  67.8 us
    unnamed x1, local copies, waits for them, and re-layouts  1.57 us

profile of v2, /device:TPU:1, one launch (start us, length us, event | category | flops | bytes accessed | tf_op | source)
XLA Modules:
  0.0 69.3 jit_solution(5910127369713397823)
XLA Ops:
  0.0 67.8 %shard_map.154 = bf16[32,2048]{1,0:T(8,128)(2,1)} custom-call(bf16[32,2048]{1,0:T(8,128)(2,1)} %lat_ref.1, bf16[64,2048]{1,0:T(8,128)(2,1)} %ctx_ref.1, f32[1,2048]{1,0:T(1,128)} %bitcast.9, f32[1,2048]{1,0:T(1,128)} %bitcast.10, bf16[512,1536]{1,0:T(8,128)(2,1)} %w_mod_ref.1, bf16[512,256]{1,0:T(8,128)(2,1)} %w_recept_ref.1, bf16[512,256]{1,0:T(8,128)(2,1)} %w_key_ref.1, ...), custom_call_target="tpu_custom_call" | custom-call | tf_op jit(solution)/shard_map/pallas_call | solution.py:553
  67.8 1.6 %copy.18 = bf16[32,2048]{1,0:T(8,128)(2,1)} copy(bf16[32,2048]{1,0:T(8,128)(2,1)} %shard_map.154) | data formatting | bytes 262144
